TPU v7x, 256 devices: a whole 4x4x8 slice. The times are simulated.
256 devices in a mesh: ep: 64 (over z, y, core), tp: 4 (over x).
Axes of the slice: x: 4, y: 4, z: 8, core: 2. Of those that a mesh axis runs over, the one named last changes fastest.
Arguments:
- cell_query_rows: bfloat16 [16384, 2048], P('ep', 'tp'), may hold values from -6 to 6
- cell_key_rows: bfloat16 [16384, 2048], P('ep', 'tp'), may hold values from -6 to 6
- cell_value_rows: bfloat16 [16384, 2048], P('ep', 'tp'), may hold values from -6 to 6
- output_gate_logits: bfloat16 [16384, 2048], P('ep', 'tp'), may hold values from -8 to 8
- log_input_gate: float32 [8, 16384], P('tp', 'ep'), may hold values from -4 to 110
- forget_gate_logits: float32 [8, 16384], P('tp', 'ep'), may hold values from -1 to 25
- extra_log_forget: float32 [8, 16384], P('tp', 'ep'), may hold values from -0.7 to 0
- cell_output_scale: float32 [2048], P('tp'), may hold values from 0.1 to 1.9
- tokens_into_experts: bfloat16 [32768, 2048], P(('ep', 'tp')), may hold values from -6 to 6
- expert_norm_scale: float32 [2048], replicated, may hold values from 0.1 to 1.9
- token_expert_index: int32 [32768, 2], P(('ep', 'tp')), may hold values from 0 to 63, all different within a row; in each aligned block of 128 rows (0 to 127, 128 to 255, ...) at most 5 rows name the same one
- chosen_expert_weight: float32 [32768, 2], P(('ep', 'tp')), may hold values from 0.3 to 3
- expert_gate_weight: bfloat16 [64, 2048, 3584], P('ep', None, 'tp'), may hold values from -0.125 to 0.125
- expert_up_weight: bfloat16 [64, 2048, 3584], P('ep', None, 'tp'), may hold values from -0.125 to 0.125
- expert_down_weight: bfloat16 [64, 3584, 2048], P('ep', 'tp'), may hold values from -0.09375 to 0.09375
Outputs:
- gated_head_output: bfloat16 [16384, 2048], P('ep', 'tp')
- expert_output: bfloat16 [32768, 2048], P(('ep', 'tp'))
Inputs may be any that keep to these rules, and one draw needn't show every extreme that they name: `token_expert_index`: each row names 2 different experts. Among the rows of one device (aligned blocks of 128 rows) no expert is named by more than 5 rows, and in every draw some expert is named by exactly 5 rows of some device.
All inputs are finite; a program needn't handle non-finite values.
Results may differ from a plain program's by a relative error of at most 0.012.
Values may be sent and summed in bfloat16 or wider, within the bound.
No kernel may reach another device: no remote copies, remote signals or barrier semaphores. Data moves between devices by JAX's collectives and lax.ppermute only.
A program may use at most 128 MiB of HBM per device.

v0:
```python
import jax
import jax.numpy as jnp
from jax import lax
from jax.sharding import Mesh
from jax.sharding import PartitionSpec as P

HEAD_DIM = 256
BLOCK = 64
TOPK = 2
EP = ("ep_0", "ep_1", "ep_2")
EP_TP = ("ep_0", "ep_1", "ep_2", "tp")
EPSILON = 1e-06
PRECISE = lax.Precision.HIGHEST


def nothing_yet(x, identity):
    return jax.tree.map(
        lambda part, zero: jnp.zeros_like(part) + jnp.asarray(zero, part.dtype), x, identity
    )


def collected_together(x, axis):
    leaves = jax.tree.leaves(x)
    turns = sorted(range(len(leaves)), key=lambda k: -leaves[k].size)
    width = (1, *leaves[turns[0]].shape)[-1]
    lines = [
        jnp.pad(leaves[k].reshape(-1), (0, -leaves[k].size % width)).reshape(-1, width)
        for k in turns
    ]
    both, at, found = (lax.all_gather(jnp.concatenate(lines), axis), 0, {})
    for k, line in zip(turns, lines):
        share = both[:, at : at + len(line)].reshape(len(both), -1)
        found[k] = share[:, : leaves[k].size].reshape(-1, *leaves[k].shape)
        at += len(line)
    numbers = iter(range(len(leaves)))
    return jax.tree.map(lambda _: found[next(numbers)], x)


def entering(x, axes, combine, identity):
    before = start = nothing_yet(x, identity)
    so_far = x
    for axis in reversed(axes):
        size, here = (lax.axis_size(axis), lax.axis_index(axis))
        pieces = collected_together(so_far, axis)
        inside, so_far = (start, start)
        for k in range(size):
            passed = k < here
            so_far = combine(so_far, jax.tree.map(lambda part: part[k], pieces))
            inside = jax.tree.map(lambda new, old: jnp.where(passed, new, old), so_far, inside)
        before = combine(inside, before)
    return before


def split_up(x, dim, size):
    before, after = (x.shape[:dim], x.shape[dim + 1 :])
    return jnp.moveaxis(x.reshape(*before, size, -1, *after), dim, 0)


def sum_at_owner(x, axis, dim):
    size = lax.axis_size(axis)
    blocks = lax.all_to_all(split_up(x, dim, size), axis, 0, 0, tiled=True)
    return jnp.sum(blocks.astype(jnp.float32), axis=0)


def combine(earlier, later):
    cell_early, norm_early, stab_early, total_early = earlier
    cell_late, norm_late, stab_late, total_late = later
    stabilizer = jnp.maximum(total_late + stab_early, stab_late)
    keep_factor = jnp.exp(total_late + stab_early - stabilizer)
    take_factor = jnp.exp(stab_late - stabilizer)
    cell_state = (
        keep_factor[..., None, None] * cell_early + take_factor[..., None, None] * cell_late
    )
    norm_state = keep_factor[..., None] * norm_early + take_factor[..., None] * norm_late
    return (cell_state, norm_state, stabilizer, total_early + total_late)


def mix_heads(
    cell_query_rows,
    cell_key_rows,
    cell_value_rows,
    output_gate_logits,
    log_input_gate,
    forget_gate_logits,
    extra_log_forget,
    cell_output_scale,
):
    n_tok, row_width = cell_query_rows.shape
    head_count = row_width // HEAD_DIM
    block_count = n_tok // BLOCK
    key_scale = HEAD_DIM ** (-0.5)
    block_shape = (block_count, BLOCK, head_count, HEAD_DIM)
    query_blocks = cell_query_rows.reshape(block_shape)
    key_blocks = cell_key_rows.reshape(block_shape)
    value_blocks = cell_value_rows.reshape(block_shape)
    gate_input = log_input_gate.reshape(head_count, block_count, BLOCK)
    forget_gate_value = (jax.nn.log_sigmoid(forget_gate_logits) + extra_log_forget).reshape(
        head_count, block_count, BLOCK
    )
    cumulative = jnp.cumsum(forget_gate_value, axis=-1)
    block_last = cumulative[..., -1]
    growth = block_last[..., None] - cumulative + gate_input
    block_top = jnp.max(growth, axis=-1)
    shares = jnp.exp(growth - block_top[..., None])
    key_float = key_blocks.astype(jnp.float32) * key_scale
    value_weighted = value_blocks.astype(jnp.float32) * shares.transpose(1, 2, 0)[..., None]
    cell_terms = jnp.einsum("bshv,bshk->bhvk", value_weighted, key_float, precision=PRECISE)
    norm_terms = jnp.einsum("hbs,bshk->bhk", shares, key_float, precision=PRECISE)
    block_terms = (cell_terms, norm_terms, block_top.T, block_last.T)
    identity_state = (
        jnp.zeros((head_count, HEAD_DIM, HEAD_DIM), jnp.float32),
        jnp.zeros((head_count, HEAD_DIM), jnp.float32),
        jnp.full((head_count,), -1e30, jnp.float32),
        jnp.zeros((head_count,), jnp.float32),
    )

    def fold_step(running, block_term):
        return (combine(running, block_term), running)

    device_total, before = lax.scan(fold_step, identity_state, block_terms)
    prior_state = entering(device_total, EP, combine, identity_state)
    zero_state = (
        jnp.zeros((head_count, HEAD_DIM, HEAD_DIM), jnp.float32),
        jnp.zeros((head_count, HEAD_DIM), jnp.float32),
        jnp.zeros((head_count,), jnp.float32),
        jnp.zeros((head_count,), jnp.float32),
    )
    start_state = combine(zero_state, prior_state)
    cell_state, norm_state, stabilizer, _ = combine(start_state, before)
    inter_log = cumulative + stabilizer.T[:, :, None]
    causal = jnp.tril(jnp.ones((BLOCK, BLOCK), dtype=bool))
    spread = jnp.where(
        causal,
        cumulative[..., :, None] - cumulative[..., None, :] + gate_input[..., None, :],
        -jnp.inf,
    )
    row_top = jnp.maximum(inter_log, jnp.max(spread, axis=-1))
    intra_weight = jnp.exp(spread - row_top[..., None])
    inter_weight = jnp.exp(inter_log - row_top)
    scores = (
        jnp.einsum("bthd,bshd->hbts", query_blocks, key_blocks, preferred_element_type=jnp.float32)
        * key_scale
        * intra_weight
    )
    weights = scores.astype(jnp.bfloat16)
    numerator = jnp.einsum(
        "hbts,bshd->hbtd", weights, value_blocks, preferred_element_type=jnp.float32
    )
    query_float = query_blocks.astype(jnp.float32)
    numerator = numerator + inter_weight[..., None] * jnp.einsum(
        "bhvk,bthk->hbtv", cell_state, query_float, precision=PRECISE
    )
    denominator = jnp.sum(scores, axis=-1) + inter_weight * jnp.einsum(
        "bhk,bthk->hbt", norm_state, query_float, precision=PRECISE
    )
    cell_out = numerator / jnp.maximum(jnp.abs(denominator), 1.0)[..., None]
    cell_out = cell_out.transpose(1, 2, 0, 3).reshape(n_tok, row_width)
    return (
        cell_out * cell_output_scale * jax.nn.sigmoid(output_gate_logits.astype(jnp.float32))
    ).astype(jnp.bfloat16)


def slot_tables(ids, experts, capacity):
    flat_ids = ids.reshape(-1)
    onehot = (flat_ids[:, None] == jnp.arange(experts, dtype=jnp.int32)[None, :]).astype(jnp.int32)
    earlier = jnp.cumsum(onehot, axis=0) - onehot
    rank_in = jnp.sum(earlier * onehot, axis=1)
    slot_index = flat_ids * capacity + rank_in
    token_of = jnp.arange(flat_ids.shape[0], dtype=jnp.int32) // ids.shape[1]
    slot_hit = slot_index[:, None] == jnp.arange(experts * capacity, dtype=jnp.int32)[None, :]
    slot_owner = jnp.sum(jnp.where(slot_hit, token_of[:, None] + 1, 0), axis=0)
    return (slot_owner, slot_index.reshape(ids.shape))


def local(
    cell_query_rows,
    cell_key_rows,
    cell_value_rows,
    output_gate_logits,
    log_input_gate,
    forget_gate_logits,
    extra_log_forget,
    cell_output_scale,
    tokens_into_experts,
    expert_norm_scale,
    token_expert_index,
    chosen_expert_weight,
    expert_gate_weight,
    expert_up_weight,
    expert_down_weight,
):
    gated_head_output = mix_heads(
        cell_query_rows,
        cell_key_rows,
        cell_value_rows,
        output_gate_logits,
        log_input_gate,
        forget_gate_logits,
        extra_log_forget,
        cell_output_scale,
    )
    ep_count = lax.axis_size(EP)
    n_tok = tokens_into_experts.shape[0]
    experts = ep_count * expert_gate_weight.shape[0]
    capacity = n_tok * TOPK * 5 // (4 * experts)
    input_float = tokens_into_experts.astype(jnp.float32)
    normed = (
        input_float
        * lax.rsqrt(jnp.mean(input_float * input_float, axis=-1, keepdims=True) + EPSILON)
        * expert_norm_scale
    ).astype(jnp.bfloat16)
    gate_matrix = expert_gate_weight[0]
    up_matrix = expert_up_weight[0]
    down_matrix = expert_down_weight[0]
    slot_owner, slot_index = slot_tables(token_expert_index, experts, capacity)
    sendbuf = jnp.where(
        (slot_owner > 0)[:, None],
        normed[jnp.maximum(slot_owner - 1, 0)],
        jnp.zeros((), jnp.bfloat16),
    )
    arrived = lax.all_to_all(sendbuf, EP, split_axis=0, concat_axis=0, tiled=True)
    routed_rows = lax.all_gather(arrived, "tp", axis=0, tiled=True)
    gate_out = jnp.dot(routed_rows, gate_matrix, preferred_element_type=jnp.float32)
    up_out = jnp.dot(routed_rows, up_matrix, preferred_element_type=jnp.float32)
    hidden = (jax.nn.silu(gate_out) * up_out).astype(jnp.bfloat16)
    summed = sum_at_owner(
        jnp.dot(hidden, down_matrix, preferred_element_type=jnp.float32).astype(jnp.bfloat16),
        "tp",
        0,
    ).astype(jnp.bfloat16)
    returned = lax.all_to_all(summed, EP, split_axis=0, concat_axis=0, tiled=True)
    picked = returned[slot_index]
    expert_output = jnp.sum(
        chosen_expert_weight[..., None] * picked.astype(jnp.float32), axis=1
    ).astype(jnp.bfloat16)
    return (gated_head_output, expert_output)


def solution(mesh):
    finer = Mesh(mesh.devices.reshape(8, 4, 2, mesh.shape["tp"]), ("ep_0", "ep_1", "ep_2", "tp"))
    placed = (
        P(EP, "tp"),
        P(EP, "tp"),
        P(EP, "tp"),
        P(EP, "tp"),
        P("tp", EP),
        P("tp", EP),
        P("tp", EP),
        P("tp"),
        P(EP_TP, None),
        P(),
        P(EP_TP, None),
        P(EP_TP, None),
        P(EP, None, "tp"),
        P(EP, None, "tp"),
        P(EP, "tp", None),
    )
    return jax.shard_map(
        local, mesh=finer, in_specs=placed, out_specs=(P(EP, "tp"), P(EP_TP, None)), check_vma=False
    )
```

profile of v0, /device:TPU:8, one launch (start us, length us, event | category | flops | bytes accessed | tf_op | source)
XLA Modules:
  0.0 352.7 jit_solution(4525034145210452684)
XLA Ops:
  7.3 0.8 add.1943
  8.0 0.7 fusion.67
  8.9 0.5 reduce_window_sum.28
  9.8 1.0 reshape.3327
  11.0 1.0 reshape.3325
  12.4 2.0 fusion.38
  14.4 17.1 %while.25 = (s32[]{:T(128)}, f32[2,256,256]{2,1,0:T(8,128)S(1)}, f32[2,256]{1,0:T(2,128)S(1)}, f32[2]{0:T(128)S(1)}, f32[2]{0:T(128)S(1)}, /*index=5*/f32[4,2,25...) while((s32[]{:T(128)}, f32[2,256,256]{2,1,0:T(8,128)S(1)}, ...), condition=%wide.region_3.4_spmd.clone, body=%wide.region_2.3_spmd.clone.sunk | while | flops 657939 | bytes 2632044 | solution.py:120
  14.4 0.9 bitcast_dynamic-update-slice_fusion.4
  15.5 0.6 bitcast_dynamic-update-slice_fusion.5
  16.1 1.3 dynamic_update_slice.27
  17.4 1.3 dynamic_update_slice.28
  18.7 0.9 bitcast_dynamic-update-slice_fusion.4
  19.7 0.6 bitcast_dynamic-update-slice_fusion.5
  20.4 1.3 dynamic_update_slice.27
  21.7 1.3 dynamic_update_slice.28
  23.0 0.9 bitcast_dynamic-update-slice_fusion.4
  24.0 0.6 bitcast_dynamic-update-slice_fusion.5
  24.7 1.3 dynamic_update_slice.27
  26.0 1.3 dynamic_update_slice.28
  27.3 0.8 bitcast_dynamic-update-slice_fusion.4
  28.3 0.6 bitcast_dynamic-update-slice_fusion.5
  29.0 1.3 dynamic_update_slice.27
  30.3 1.3 dynamic_update_slice.28
  31.6 0.8 maximum_bitcast_fusion
  33.1 0.6 reduce-window.6
  34.4 15.4 %all-gather.13.cloned.1.call-done = f32[2,516,256]{2,1,0:T(8,128)} async-done(((f32[1,516,256]{2,1,0:T(8,128)}), f32[2,516,256]{2,1,0:T(8,128)}) %all-gather.13.cloned.1.call-update) | async-done | bytes 1056784 | tf_op jit(solution)/shard_map/all_gather | solution.py:30
  49.9 0.8 fusion.135
  51.2 0.8 broadcast_bitcast_fusion.11
  52.0 1.5 fusion.34
  53.6 0.8 maximum_bitcast_fusion.1
  54.5 2.4 gather_fusion
  57.0 0.6 gather.9
  58.0 61.6 %all_to_all.26 = bf16[64,5,2048]{2,1,0:T(8,128)(2,1)S(1)} all-to-all(bf16[64,5,2048]{2,1,0:T(8,128)(2,1)S(1)} %broadcast_select_fusion.3), channel_id=1, replica_groups=mesh['ep_0'=8,'ep_1'=4,'ep_2'=2,'tp'=4] {'ep_0','ep_1','ep_2'}, dimensions={0} | all-to-all | bytes 2621440 | tf_op jit(solution)/shard_map/all_to_all | solution.py:221
  119.6 1.4 all_to_all.18
  121.3 0.8 fusion.133
  122.2 0.6 subtract_exponential_fusion.18
  122.9 0.8 broadcast_bitcast_fusion.7
  123.9 2.0 fusion.27
  125.9 0.9 maximum_bitcast_fusion.2
  126.8 49.9 %all-gather.11.cloned.1.call-done = bf16[1280,2048]{1,0:T(8,128)(2,1)} async-done(((bf16[320,2048]{1,0:T(8,128)(2,1)}), bf16[1280,2048]{1,0:T(8,128)(2,1)}) %all-gather.11.cloned.1.call-update) | async-done | bytes 5242896 | tf_op jit(solution)/shard_map/all_gather | solution.py:222
  176.7 9.9 %fusion.11 = f32[1280,896]{1,0:T(8,128)} fusion(bf16[1280,2048]{1,0:T(8,128)(2,1)} %all-gather.11.cloned.1.call-done, bf16[1,2048,896]{2,1,0:T(8,128)(2,1)} %param.29), kind=kOutput, calls=%fused_computation.26 | convolution fusion | flops 4697620480 | bytes 13500416 | tf_op jit(solution)/shard_map/dot_general | solution.py:223
  186.7 17.7 %convolution_convert_fusion = bf16[1280,2048]{1,0:T(8,128)(2,1)} fusion(bf16[1,896,2048]{2,1,0:T(8,128)(2,1)} %param.31, f32[1280,896]{1,0:T(8,128)} %fusion.11, bf16[1280,2048]{1,0:T(8,128)(2,1)} %all-gather.11.cloned.1.call-done, bf16[1,2048,896]{2,1,0:T(8,128)(2,1)} %param.30), kind=kOutput, calls=%fused_computation.22 | convolution fusion | flops 9404743680 | bytes 22413312 | tf_op jit(solution)/shard_map/dot_general | solution.py:227
  204.4 5.2 %all-to-all-start.1 = ((bf16[4,320,2048]{2,1,0:T(8,128)(2,1)}), bf16[4,320,2048]{2,1,0:T(8,128)(2,1)}, u32[]{:S(2)}, u32[]{:S(2)}) async-start(bf16[4,320,2048]{2,1,0:T(8,128)(2,1)} %bitcast.529), calls=%async_computation.1 | async-start | bytes 10485760 | tf_op jit(solution)/shard_map/all_to_all | solution.py:61
  209.8 0.8 reshape.3324
  210.6 0.7 compare_select_fusion.1
  211.6 0.8 copy.148
  212.6 1.0 fusion.134
  213.9 1.4 fusion.132
  215.3 19.0 %all-gather.17.cloned.1.call-done = f32[8,516,256]{2,1,0:T(8,128)} async-done(((f32[1,516,256]{2,1,0:T(8,128)}), f32[8,516,256]{2,1,0:T(8,128)}) %all-gather.17.cloned.1.call-update) | async-done | bytes 4227088 | tf_op jit(solution)/shard_map/all_gather | solution.py:30
  234.3 0.9 fusion.131
  235.9 1.0 add_bitcast_fusion.2
  236.9 32.8 %all-to-all-done.1 = bf16[4,320,2048]{2,1,0:T(8,128)(2,1)} async-done(((bf16[4,320,2048]{2,1,0:T(8,128)(2,1)}), bf16[4,320,2048]{2,1,0:T(8,128)(2,1)}, u32[]{:S(2)}, u32[]{:S(2)}) %all-to-all-start.1) | async-done | bytes 5242912 | tf_op jit(solution)/shard_map/all_to_all | solution.py:61
  269.7 3.6 %reduce_sum.66 = bf16[320,2048]{1,0:T(8,128)(2,1)S(1)} reduce(bf16[4,320,2048]{2,1,0:T(8,128)(2,1)} %all-to-all-done.1, bf16[]{:T(256)} %constant.113.clone.1), dimensions={0}, to_apply=%region_11.12 | reduce | flops 1966080 | bytes 6553602 | tf_op jit(solution)/shard_map/reduce_sum | solution.py:62
  273.3 1.6 all_to_all.20
  275.0 10.7 %all-to-all-start.2 = ((bf16[64,5,2048]{2,1,0:T(8,128)(2,1)}), bf16[64,5,2048]{2,1,0:T(8,128)(2,1)S(1)}, u32[]{:S(2)}, u32[]{:S(2)}) async-start(bf16[64,5,2048]{2,1,0:T(8,128)(2,1)} %all_to_all.20), calls=%async_computation.2 | async-start | bytes 4194304 | tf_op jit(solution)/shard_map/all_to_all | solution.py:231
  286.5 2.8 fusion.130
  289.5 1.4 multiply_add_fusion.1
  291.1 1.5 fusion.20
  293.5 0.9 multiply_convert_fusion.1
  294.4 42.5 %all-to-all-done.2 = bf16[64,5,2048]{2,1,0:T(8,128)(2,1)S(1)} async-done(((bf16[64,5,2048]{2,1,0:T(8,128)(2,1)}), bf16[64,5,2048]{2,1,0:T(8,128)(2,1)S(1)}, u32[]{:S(2)}, u32[]{:S(2)}) %all-to-all-start.2) | async-done | bytes 1310752 | tf_op jit(solution)/shard_map/all_to_all | solution.py:231
  336.9 0.6 all_to_all.22
  337.5 2.4 gather_fusion.1
  339.9 2.4 reshape.3367
  342.2 3.9 %multiply_reduce_fusion = bf16[128,2048]{1,0:T(8,128)(2,1)} fusion(f32[128,2,2048]{2,1,0:T(2,128)S(1)} %reshape.3367, f32[128,2]{1,0:T(8,128)S(1)} %copy.148), kind=kLoop, calls=%fused_computation.30 | loop fusion | flops 786432 | bytes 2622464 | tf_op jit(solution)/shard_map/reduce_sum | solution.py:233
  (233 shorter events, 8.1 us)
Async XLA Ops:
  7.2 42.7 %all-gather.13.cloned.1.call-start = ((), (), s32[]{:S(2)}) async-start(), calls=%async_computation.4 | async-start | bytes 1597440 | tf_op jit(solution)/shard_map/all_gather | solution.py:30
  10.9 3.6 %copy-start.10 = (bf16[4,64,2,256]{3,2,1,0:T(2,128)(2,1)}, bf16[4,64,2,256]{3,2,1,0:T(2,128)(2,1)S(1)}, u32[]{:S(2)}) copy-start(bf16[4,64,2,256]{3,2,1,0:T(2,128)(2,1)S(1)} %reshape.3327) | copy-start | bytes 786436
  12.0 2.4 copy-start.12
  14.4 18.1 %copy-start.54 = (s32[128,2]{0,1:T(2,128)S(1)}, s32[128,2]{0,1:T(2,128)}, u32[]{:S(2)}) copy-start(s32[128,2]{0,1:T(2,128)} %param.27) | copy-start | bytes 3076
  31.5 1.3 copy-start.2
  31.5 2.7 copy-start.17
  32.4 88.8 %all-gather.15.cloned.1.call-start = ((), (), s32[]{:S(2)}) async-start(), calls=%async_computation.5 | async-start | bytes 2662400 | tf_op jit(solution)/shard_map/all_gather | solution.py:30
  50.7 3.7 %copy-start.32 = (f32[2]{0:T(128)}, f32[2]{0:T(128)S(1)}, u32[]{:S(2)}) copy-start(f32[2]{0:T(128)S(1)} %get-tuple-element.244) | copy-start | bytes 28
  50.7 3.8 %copy-start.41 = (f32[2]{0:T(128)}, f32[2]{0:T(128)S(1)}, u32[]{:S(2)}) copy-start(f32[2]{0:T(128)S(1)} %get-tuple-element.245) | copy-start | bytes 28
  50.7 3.8 %copy-start.36 = (f32[2]{0:T(128)}, f32[2]{0:T(128)S(1)}, u32[]{:S(2)}) copy-start(f32[2]{0:T(128)S(1)} %get-tuple-element.324) | copy-start | bytes 28
  50.7 3.8 %copy-start.38 = (f32[2]{0:T(128)}, f32[2]{0:T(128)S(1)}, u32[]{:S(2)}) copy-start(f32[2]{0:T(128)S(1)} %get-tuple-element.325) | copy-start | bytes 28
  50.8 6.2 %copy-start.34 = (f32[2]{0:T(128)}, f32[2]{0:T(128)S(1)}, u32[]{:S(2)}) copy-start(f32[2]{0:T(128)S(1)} %get-tuple-element.299) | copy-start | bytes 28
  54.4 122.3 %all-gather.11.cloned.1.call-start = ((), (), s32[]{:S(2)}) async-start(), calls=%async_computation.3 | async-start | bytes 6553600 | tf_op jit(solution)/shard_map/all_gather | solution.py:222
  121.0 113.3 %all-gather.17.cloned.1.call-start = ((), (), s32[]{:S(2)}) async-start(), calls=%async_computation.6 | async-start | bytes 4792320 | tf_op jit(solution)/shard_map/all_gather | solution.py:30
  122.1 1.7 copy-start.24
  122.1 1.7 copy-start.43
  122.2 1.7 copy-start.46
  122.2 1.7 copy-start.48
  122.2 1.7 copy-start.50
  122.8 1.0 copy-start.26
  122.8 1.1 copy-start.28
  122.8 1.1 copy-start.30
  122.8 1.0 copy-start.18
  122.8 1.0 copy-start.20
  122.9 1.0 copy-start.22
  204.4 5.4 %copy-start.15 = (bf16[256,512]{1,0:T(8,128)(2,1)S(1)}, bf16[256,512]{1,0:T(8,128)(2,1)}, u32[]{:S(2)}) copy-start(bf16[256,512]{1,0:T(8,128)(2,1)} %param.17) | copy-start | bytes 786436
  204.4 8.2 %copy-start.1 = (f32[2,516,256]{2,1,0:T(8,128)S(1)}, f32[2,516,256]{2,1,0:T(8,128)}, u32[]{:S(2)}) copy-start(f32[2,516,256]{2,1,0:T(8,128)} %all-gather.13.cloned.1.call-done) | copy-start | bytes 3170308
  204.4 65.3 %all-to-all-start.1 = ((bf16[4,320,2048]{2,1,0:T(8,128)(2,1)}), bf16[4,320,2048]{2,1,0:T(8,128)(2,1)}, u32[]{:S(2)}, u32[]{:S(2)}) async-start(bf16[4,320,2048]{2,1,0:T(8,128)(2,1)} %bitcast.529), calls=%async_computation.1 | async-start | bytes 10485760 | tf_op jit(solution)/shard_map/all_to_all | solution.py:61
  209.6 4.1 %copy-start = (f32[4,516,256]{2,1,0:T(8,128)S(1)}, f32[4,516,256]{2,1,0:T(8,128)}, u32[]{:S(2)}) copy-start(f32[4,516,256]{2,1,0:T(8,128)} %all-gather.15.cloned.1.call-done) | copy-start | bytes 6340612
  213.7 21.6 %copy-start.40 = (f32[4,2]{1,0:T(4,128)S(1)}, f32[4,2]{1,0:T(4,128)}, u32[]{:S(2)}) copy-start(f32[4,2]{1,0:T(4,128)} %get-tuple-element.81) | copy-start | bytes 100
  213.7 21.7 %copy-start.56 = (f32[4,2]{1,0:T(4,128)S(1)}, f32[4,2]{1,0:T(4,128)}, u32[]{:S(2)}) copy-start(f32[4,2]{1,0:T(4,128)} %get-tuple-element.76) | copy-start | bytes 100
  213.7 21.9 %copy-start.42 = (f32[2]{0:T(128)S(1)}, f32[2]{0:T(128)}, u32[]{:S(2)}) copy-start(f32[2]{0:T(128)} %copy-done.41) | copy-start | bytes 28
  213.7 21.9 %copy-start.44 = (f32[2]{0:T(128)S(1)}, f32[2]{0:T(128)}, u32[]{:S(2)}) copy-start(f32[2]{0:T(128)} %copy-done.43) | copy-start | bytes 28
  213.7 21.9 %copy-start.47 = (f32[2]{0:T(128)S(1)}, f32[2]{0:T(128)}, u32[]{:S(2)}) copy-start(f32[2]{0:T(128)} %copy-done.46) | copy-start | bytes 28
  213.7 21.9 %copy-start.49 = (f32[2]{0:T(128)S(1)}, f32[2]{0:T(128)}, u32[]{:S(2)}) copy-start(f32[2]{0:T(128)} %copy-done.48) | copy-start | bytes 28
  213.7 21.9 %copy-start.51 = (f32[2]{0:T(128)S(1)}, f32[2]{0:T(128)}, u32[]{:S(2)}) copy-start(f32[2]{0:T(128)} %copy-done.50) | copy-start | bytes 28
  213.7 21.9 %copy-start.53 = (f32[2]{0:T(128)S(1)}, f32[2]{0:T(128)}, u32[]{:S(2)}) copy-start(f32[2]{0:T(128)} %copy-done.52) | copy-start | bytes 28
  213.7 21.9 %copy-start.57 = (f32[2]{0:T(128)S(1)}, f32[2]{0:T(128)}, u32[]{:S(2)}) copy-start(f32[2]{0:T(128)} %get-tuple-element.292) | copy-start | bytes 28
  213.7 21.9 %copy-start.58 = (f32[2]{0:T(128)S(1)}, f32[2]{0:T(128)}, u32[]{:S(2)}) copy-start(f32[2]{0:T(128)} %get-tuple-element.293) | copy-start | bytes 28
  213.7 22.0 %copy-start.19 = (f32[2]{0:T(128)S(1)}, f32[2]{0:T(128)}, u32[]{:S(2)}) copy-start(f32[2]{0:T(128)} %copy-done.18) | copy-start | bytes 28
  213.8 22.0 %copy-start.21 = (f32[2]{0:T(128)S(1)}, f32[2]{0:T(128)}, u32[]{:S(2)}) copy-start(f32[2]{0:T(128)} %copy-done.20) | copy-start | bytes 28
  213.8 22.0 %copy-start.23 = (f32[2]{0:T(128)S(1)}, f32[2]{0:T(128)}, u32[]{:S(2)}) copy-start(f32[2]{0:T(128)} %copy-done.22) | copy-start | bytes 28
  213.8 22.0 %copy-start.25 = (f32[2]{0:T(128)S(1)}, f32[2]{0:T(128)}, u32[]{:S(2)}) copy-start(f32[2]{0:T(128)} %copy-done.24) | copy-start | bytes 28
  213.8 22.0 %copy-start.27 = (f32[2]{0:T(128)S(1)}, f32[2]{0:T(128)}, u32[]{:S(2)}) copy-start(f32[2]{0:T(128)} %copy-done.26) | copy-start | bytes 28
  213.8 22.0 %copy-start.29 = (f32[2]{0:T(128)S(1)}, f32[2]{0:T(128)}, u32[]{:S(2)}) copy-start(f32[2]{0:T(128)} %copy-done.28) | copy-start | bytes 28
  213.8 22.0 %copy-start.31 = (f32[2]{0:T(128)S(1)}, f32[2]{0:T(128)}, u32[]{:S(2)}) copy-start(f32[2]{0:T(128)} %copy-done.30) | copy-start | bytes 28
  213.8 22.0 %copy-start.33 = (f32[2]{0:T(128)S(1)}, f32[2]{0:T(128)}, u32[]{:S(2)}) copy-start(f32[2]{0:T(128)} %copy-done.32) | copy-start | bytes 28
  213.8 22.0 %copy-start.35 = (f32[2]{0:T(128)S(1)}, f32[2]{0:T(128)}, u32[]{:S(2)}) copy-start(f32[2]{0:T(128)} %copy-done.34) | copy-start | bytes 28
  213.8 22.0 %copy-start.37 = (f32[2]{0:T(128)S(1)}, f32[2]{0:T(128)}, u32[]{:S(2)}) copy-start(f32[2]{0:T(128)} %copy-done.36) | copy-start | bytes 28
  213.8 22.0 %copy-start.39 = (f32[2]{0:T(128)S(1)}, f32[2]{0:T(128)}, u32[]{:S(2)}) copy-start(f32[2]{0:T(128)} %copy-done.38) | copy-start | bytes 28
  213.9 23.0 %copy-start.45 = (f32[4,2,256]{2,1,0:T(2,128)S(1)}, f32[4,2,256]{2,1,0:T(2,128)}, u32[]{:S(2)}) copy-start(f32[4,2,256]{2,1,0:T(2,128)} %get-tuple-element.83) | copy-start | bytes 24580
  275.0 10.8 %copy-start.14 = (bf16[4,64,2,256]{3,2,1,0:T(2,128)(2,1)S(1)}, bf16[4,64,2,256]{3,2,1,0:T(2,128)(2,1)}, u32[]{:S(2)}) copy-start(bf16[4,64,2,256]{3,2,1,0:T(2,128)(2,1)} %reshape.3324) | copy-start | bytes 786436
  275.0 11.1 %copy-start.13 = (bf16[4,64,2,256]{3,2,1,0:T(2,128)(2,1)S(1)}, bf16[4,64,2,256]{3,2,1,0:T(2,128)(2,1)}, u32[]{:S(2)}) copy-start(bf16[4,64,2,256]{3,2,1,0:T(2,128)(2,1)} %copy-done.12) | copy-start | bytes 786436
  275.0 61.9 %all-to-all-start.2 = ((bf16[64,5,2048]{2,1,0:T(8,128)(2,1)}), bf16[64,5,2048]{2,1,0:T(8,128)(2,1)S(1)}, u32[]{:S(2)}, u32[]{:S(2)}) async-start(bf16[64,5,2048]{2,1,0:T(8,128)(2,1)} %all_to_all.20), calls=%async_computation.2 | async-start | bytes 4194304 | tf_op jit(solution)/shard_map/all_to_all | solution.py:231
  286.4 2.8 copy-start.3
  286.4 2.8 copy-start.4
  286.4 2.8 copy-start.6
  286.4 2.8 copy-start.7
  286.5 2.9 copy-start.8
  286.5 3.1 copy-start.9
  289.5 1.6 copy-start.5
  291.0 1.6 copy-start.11
  292.6 1.0 copy-start.16
  292.6 0.9 copy-start.55
  (1 other events, 0.5 us)
Sparse Core Ops, SparseCore 0:
  32.5 17.2 all-gather.12
  54.5 50.8 all-gather.14
  121.1 55.5 all-gather.10
  178.4 55.8 all-gather.16
where the time goes:
time: 354 us; the launch traced here: 353 us
  waiting for transfers between devices  160 us (45%)
  blocking collectives  61.6 us (17%)
  local copies, waits for them, and re-layouts  37.3 us (11%)
  matrix products  32.3 us (9%)
  other arithmetic  30.3 us (9%)
  starting transfers between devices  16.3 us (5%)
  between operations  15.1 us (4%)
    all_to_all x1, blocking collectives, local(): lax.all_to_all(sendbuf, EP, split_axis=0, concat_axis=0, tiled=True)  61.6 us
    all_gather x1, waiting for transfers between devices, local(): routed_rows = lax.all_gather(arrived, 'tp', axis=0, tiled=True)  49.9 us
    all_to_all x1, waiting for transfers between devices, local(): lax.all_to_all(summed, EP, split_axis=0, concat_axis=0, tiled=True)  42.5 us
    all_gather x3, waiting for transfers between devices, collected_together(): both, at, found = (lax.all_gather(jnp.concatenate(lines), axis), 0, {})  34.5 us
    all_to_all x1, waiting for transfers between devices, sum_at_owner(): blocks = lax.all_to_all(split_up(x, dim, size), axis, 0, 0, tiled=True)  32.8 us
    dot_general x1, matrix products, local(): jnp.dot(hidden, down_matrix, preferred_element_type=jnp.float32)  17.7 us
    all_to_all x1, starting transfers between devices, local(): lax.all_to_all(summed, EP, split_axis=0, concat_axis=0, tiled=True)  10.7 us
    dynamic_update_slice x8, local copies, waits for them, and re-layouts, mix_heads(): device_total, before = lax.scan(fold_step, identity_state, block_terms)  10.3 us
  transfers between devices with their start and end apart: 6, of which 5 were waited for; matrix products, arithmetic and copies ran while one was open for 15% of the time, Pallas kernels for 0%

commit v1 on v0

--- a/solution.py
+++ b/solution.py
@@ -1,3 +1,4 @@
+import functools
 import jax
 import jax.numpy as jnp
 from jax import lax
@@ -11,6 +12,34 @@
 EP_TP = ("ep_0", "ep_1", "ep_2", "tp")
 EPSILON = 1e-06
 PRECISE = lax.Precision.HIGHEST
+
+
+def advance_leaves(content, dim_k):
+    built = lax.axis_index("tp")
+    response = lax.axis_size("tp")
+    now, wide_out, seen_now = (response, built, content.shape[dim_k])
+    nodes = [(m, (m + 1) % now) for m in range(now)]
+    by_place = [(m, (m - 1) % now) for m in range(now)]
+    u_next = jnp.zeros(
+        (*content.shape[:dim_k], now * seen_now, *content.shape[dim_k + 1 :]), content.dtype
+    )
+    u_next = lax.dynamic_update_slice_in_dim(u_next, content, wide_out * seen_now, axis=dim_k)
+    tmp = long_array = content
+    moved = now // 2
+    for k0 in range(1, moved + 1):
+        tmp = lax.ppermute(tmp, perm=nodes, axis_name="tp")
+        u_next = lax.dynamic_update_slice_in_dim(
+            u_next, tmp, (wide_out - k0) % now * seen_now, axis=dim_k
+        )
+        if k0 < now - moved:
+            long_array = lax.ppermute(long_array, axis_name="tp", perm=by_place)
+            u_next = lax.dynamic_update_slice_in_dim(
+                u_next, long_array, (wide_out + k0) % now * seen_now, axis=dim_k
+            )
+    return u_next
+
+
+shape_runs = functools.partial(advance_leaves, dim_k=0)
 
 
 def nothing_yet(x, identity):
@@ -219,7 +248,7 @@
         jnp.zeros((), jnp.bfloat16),
     )
     arrived = lax.all_to_all(sendbuf, EP, split_axis=0, concat_axis=0, tiled=True)
-    routed_rows = lax.all_gather(arrived, "tp", axis=0, tiled=True)
+    routed_rows = shape_runs(arrived)
     gate_out = jnp.dot(routed_rows, gate_matrix, preferred_element_type=jnp.float32)
     up_out = jnp.dot(routed_rows, up_matrix, preferred_element_type=jnp.float32)
     hidden = (jax.nn.silu(gate_out) * up_out).astype(jnp.bfloat16)

time: 354 us -> 341 us (0.963)
  blocking collectives: 61.6 us -> 0 us
  waiting for transfers between devices: 160 us -> 179 us
  starting transfers between devices: 16.3 us -> 33.2 us
  local copies, waits for them, and re-layouts: 37.3 us -> 47 us
    all_to_all x1 -> x0, blocking collectives: 61.6 us -> none  [local(): lax.all_to_all(sendbuf, EP, split_axis=0, concat_axis=0, tiled=True)]
    all_gather x1 -> x0, waiting for transfers between devices: 49.9 us -> none  [local(): routed_rows = lax.all_gather(arrived, 'tp', axis=0, tiled=True)]
    all_to_all x0 -> x1, waiting for transfers between devices: none -> 46.5 us  [local(): lax.all_to_all(sendbuf, EP, split_axis=0, concat_axis=0, tiled=True)]
    ppermute x0 -> x3, waiting for transfers between devices: none -> 42.6 us  [the longest x2 42.6 us: advance_leaves(): tmp = lax.ppermute(tmp, perm=nodes, axis_name='tp')]
    all_gather x3, waiting for transfers between devices: 34.5 us -> 0.04 us  [collected_together(): both, at, found = (lax.all_gather(jnp.concatenate(lines), axis), 0, {})]
    all_to_all x1, waiting for transfers between devices: 32.8 us -> 51.7 us  [sum_at_owner(): blocks = lax.all_to_all(split_up(x, dim, size), axis, 0, 0, tiled=True)]
    all_to_all x0 -> x1, starting transfers between devices: none -> 12.1 us  [local(): lax.all_to_all(sendbuf, EP, split_axis=0, concat_axis=0, tiled=True)]
    dynamic_update_slice x0 -> x4, local copies, waits for them, and re-layouts: none -> 7.51 us  [the longest x2 3.71 us: advance_leaves(): lax.dynamic_update_slice_in_dim(u_next, tmp, (wide_out - k0) % now * seen...]
  transfers between devices with their start and end apart: 6 -> 9, of which waited for: 5 -> 5; matrix products, arithmetic and copies ran while one was open for 15% -> 22% of each run, Pallas kernels for 0% -> 0%
where the time goes in v1:
time: 341 us; the launch traced here: 340 us
  waiting for transfers between devices  179 us (52%)
  local copies, waits for them, and re-layouts  47 us (14%)
  matrix products  34.3 us (10%)
  starting transfers between devices  33.2 us (10%)
  other arithmetic  31.6 us (9%)
  between operations  15 us (4%)
    all_to_all x1, waiting for transfers between devices, sum_at_owner(): blocks = lax.all_to_all(split_up(x, dim, size), axis, 0, 0, tiled=True)  51.7 us
    all_to_all x1, waiting for transfers between devices, local(): lax.all_to_all(sendbuf, EP, split_axis=0, concat_axis=0, tiled=True)  46.5 us
    ppermute x2, waiting for transfers between devices, advance_leaves(): tmp = lax.ppermute(tmp, perm=nodes, axis_name='tp')  42.6 us
    all_to_all x1, waiting for transfers between devices, local(): lax.all_to_all(summed, EP, split_axis=0, concat_axis=0, tiled=True)  37.8 us
    dot_general x1, matrix products, local(): jnp.dot(hidden, down_matrix, preferred_element_type=jnp.float32)  17.6 us
    all_to_all x1, starting transfers between devices, local(): lax.all_to_all(summed, EP, split_axis=0, concat_axis=0, tiled=True)  12.2 us
    all_to_all x1, starting transfers between devices, local(): lax.all_to_all(sendbuf, EP, split_axis=0, concat_axis=0, tiled=True)  12.1 us
    dynamic_update_slice x8, local copies, waits for them, and re-layouts, mix_heads(): device_total, before = lax.scan(fold_step, identity_state, block_terms)  10.3 us
  transfers between devices with their start and end apart: 9, of which 5 were waited for; matrix products, arithmetic and copies ran while one was open for 22% of the time, Pallas kernels for 0%

profile of v1, /device:TPU:8, one launch (start us, length us, event | category | flops | bytes accessed | tf_op | source)
XLA Modules:
  0.0 340.1 jit_solution(7959544546572490662)
XLA Ops:
  7.3 0.8 add.1970
  8.0 0.7 fusion.70
  9.8 1.0 reshape.3327
  11.0 1.0 reshape.3325
  12.4 2.0 fusion.41
  14.4 17.1 %while.25 = (s32[]{:T(128)}, f32[2,256,256]{2,1,0:T(8,128)S(1)}, f32[2,256]{1,0:T(2,128)S(1)}, f32[2]{0:T(128)S(1)}, f32[2]{0:T(128)S(1)}, /*index=5*/f32[4,2,25...) while((s32[]{:T(128)}, f32[2,256,256]{2,1,0:T(8,128)S(1)}, ...), condition=%wide.region_3.4_spmd.clone, body=%wide.region_2.3_spmd.clone.sunk | while | flops 657939 | bytes 2632044 | solution.py:149
  14.4 0.8 bitcast_dynamic-update-slice_fusion.4
  16.2 1.3 dynamic_update_slice.47
  17.4 1.3 dynamic_update_slice.48
  18.7 0.8 bitcast_dynamic-update-slice_fusion.4
  20.4 1.3 dynamic_update_slice.47
  21.7 1.3 dynamic_update_slice.48
  23.0 0.8 bitcast_dynamic-update-slice_fusion.4
  24.7 1.3 dynamic_update_slice.47
  26.0 1.3 dynamic_update_slice.48
  27.3 0.8 bitcast_dynamic-update-slice_fusion.4
  29.0 1.3 dynamic_update_slice.47
  30.2 1.3 dynamic_update_slice.48
  31.6 0.8 maximum_bitcast_fusion
  34.4 2.4 gather_fusion
  37.5 1.6 broadcast_select_fusion.3
  39.2 12.1 %all-to-all-start = ((bf16[64,5,2048]{2,1,0:T(8,128)(2,1)}), bf16[64,5,2048]{2,1,0:T(8,128)(2,1)S(1)}, u32[]{:S(2)}, u32[]{:S(2)}) async-start(bf16[64,5,2048]{2,1,0:T(8,128)(2,1)} %broadcast_select_fusion.3), calls=%async_computation | async-start | bytes 4194304 | tf_op jit(solution)/shard_map/all_to_all | solution.py:250
  51.3 0.8 fusion.138
  52.7 0.8 broadcast_bitcast_fusion.11
  53.5 1.5 fusion.37
  55.1 0.8 maximum_bitcast_fusion.1
  56.0 46.5 %all-to-all-done = bf16[64,5,2048]{2,1,0:T(8,128)(2,1)S(1)} async-done(((bf16[64,5,2048]{2,1,0:T(8,128)(2,1)}), bf16[64,5,2048]{2,1,0:T(8,128)(2,1)S(1)}, u32[]{:S(2)}, u32[]{:S(2)}) %all-to-all-start) | async-done | bytes 1310752 | tf_op jit(solution)/shard_map/all_to_all | solution.py:250
  103.1 1.6 collective-permute-start
  104.7 1.7 collective-permute-start.1
  106.4 3.1 broadcast_in_dim.54
  109.5 1.2 constant_dynamic-update-slice_fusion.3
  110.6 22.7 %collective-permute-done = bf16[320,2048]{1,0:T(8,128)(2,1)S(1)} collective-permute-done((bf16[320,2048]{1,0:T(8,128)(2,1)S(1)}, bf16[320,2048]{1,0:T(8,128)(2,1)S(1)}, u32[]{:S(2)}, u32[]{:S(2)}) %collective-permute-start) | collective-permute-done | bytes 1310752 | tf_op jit(solution)/shard_map/ppermute | solution.py:30
  133.7 1.1 constant_dynamic-update-slice_fusion.2
  134.8 2.6 constant_dynamic-update-slice_fusion.1
  137.4 0.8 fusion.136
  139.0 0.8 broadcast_bitcast_fusion.7
  140.0 2.0 fusion.30
  141.9 0.9 maximum_bitcast_fusion.2
  143.0 19.9 %collective-permute-done.2 = bf16[320,2048]{1,0:T(8,128)(2,1)} collective-permute-done((bf16[320,2048]{1,0:T(8,128)(2,1)S(1)}, bf16[320,2048]{1,0:T(8,128)(2,1)}, u32[]{:S(2)}, u32[]{:S(2)}) %collective-permute-start.2) | collective-permute-done | bytes 1310752 | tf_op jit(solution)/shard_map/ppermute | solution.py:30
  162.8 2.6 constant_dynamic-update-slice_fusion
  165.4 10.0 %fusion.14 = f32[1280,896]{1,0:T(8,128)} fusion(bf16[1280,2048]{1,0:T(8,128)(2,1)} %constant_dynamic-update-slice_fusion, bf16[1,2048,896]{2,1,0:T(8,128)(2,1)} %param.29), kind=kOutput, calls=%fused_computation.27 | convolution fusion | flops 4697620480 | bytes 13500416 | tf_op jit(solution)/shard_map/dot_general | solution.py:252
  175.4 17.6 %convolution_convert_fusion = bf16[1280,2048]{1,0:T(8,128)(2,1)} fusion(bf16[1,896,2048]{2,1,0:T(8,128)(2,1)} %param.31, f32[1280,896]{1,0:T(8,128)} %fusion.14, bf16[1280,2048]{1,0:T(8,128)(2,1)} %constant_dynamic-update-slice_fusion, bf16[1,2048,896]{2,1,0:T(8,128)(2,1)} %param.30), kind=kOutput, calls=%fused_computation.22 | convolution fusion | flops 9404743680 | bytes 22413312 | tf_op jit(solution)/shard_map/dot_general | solution.py:256
  193.0 5.2 %all-to-all-start.1 = ((bf16[4,320,2048]{2,1,0:T(8,128)(2,1)}), bf16[4,320,2048]{2,1,0:T(8,128)(2,1)}, u32[]{:S(2)}, u32[]{:S(2)}) async-start(bf16[4,320,2048]{2,1,0:T(8,128)(2,1)} %bitcast.531), calls=%async_computation.1 | async-start | bytes 10485760 | tf_op jit(solution)/shard_map/all_to_all | solution.py:90
  198.4 0.8 reshape.3324
  199.3 0.7 compare_select_fusion.1
  200.2 0.8 copy.148
  201.3 1.0 fusion.137
  202.3 1.4 fusion.135
  203.7 51.7 %all-to-all-done.1 = bf16[4,320,2048]{2,1,0:T(8,128)(2,1)} async-done(((bf16[4,320,2048]{2,1,0:T(8,128)(2,1)}), bf16[4,320,2048]{2,1,0:T(8,128)(2,1)}, u32[]{:S(2)}, u32[]{:S(2)}) %all-to-all-start.1) | async-done | bytes 5242912 | tf_op jit(solution)/shard_map/all_to_all | solution.py:90
  255.4 3.6 %reduce_sum.66 = bf16[320,2048]{1,0:T(8,128)(2,1)S(1)} reduce(bf16[4,320,2048]{2,1,0:T(8,128)(2,1)} %all-to-all-done.1, bf16[]{:T(256)} %constant.134.clone.1), dimensions={0}, to_apply=%region_11.12 | reduce | flops 1966080 | bytes 6553602 | tf_op jit(solution)/shard_map/reduce_sum | solution.py:91
  259.0 1.6 all_to_all.20
  260.8 12.2 %all-to-all-start.2 = ((bf16[64,5,2048]{2,1,0:T(8,128)(2,1)}), bf16[64,5,2048]{2,1,0:T(8,128)(2,1)S(1)}, u32[]{:S(2)}, u32[]{:S(2)}) async-start(bf16[64,5,2048]{2,1,0:T(8,128)(2,1)} %all_to_all.20), calls=%async_computation.2 | async-start | bytes 4194304 | tf_op jit(solution)/shard_map/all_to_all | solution.py:260
  273.1 0.9 fusion.134
  274.6 1.0 add_bitcast_fusion.2
  275.8 1.3 fusion.54
  277.1 1.3 fusion.139
  278.5 2.8 fusion.133
  281.6 1.4 multiply_add_fusion.1
  283.2 1.5 fusion.23
  285.6 0.9 multiply_convert_fusion.1
  286.4 37.8 %all-to-all-done.2 = bf16[64,5,2048]{2,1,0:T(8,128)(2,1)S(1)} async-done(((bf16[64,5,2048]{2,1,0:T(8,128)(2,1)}), bf16[64,5,2048]{2,1,0:T(8,128)(2,1)S(1)}, u32[]{:S(2)}, u32[]{:S(2)}) %all-to-all-start.2) | async-done | bytes 1310752 | tf_op jit(solution)/shard_map/all_to_all | solution.py:260
  324.9 2.4 gather_fusion.1
  327.2 2.4 reshape.3367
  329.6 3.9 %multiply_reduce_fusion = bf16[128,2048]{1,0:T(8,128)(2,1)} fusion(f32[128,2,2048]{2,1,0:T(2,128)S(1)} %reshape.3367, f32[128,2]{1,0:T(8,128)S(1)} %copy.148), kind=kLoop, calls=%fused_computation.31 | loop fusion | flops 786432 | bytes 2622464 | tf_op jit(solution)/shard_map/reduce_sum | solution.py:262
  (240 shorter events, 13.0 us)
Async XLA Ops:
  7.2 44.2 %all-gather.10.cloned.1.call-start = ((), (), s32[]{:S(2)}) async-start(), calls=%async_computation.3 | async-start | bytes 1597440 | tf_op jit(solution)/shard_map/all_gather | solution.py:59
  10.9 3.6 %copy-start.10 = (bf16[4,64,2,256]{3,2,1,0:T(2,128)(2,1)}, bf16[4,64,2,256]{3,2,1,0:T(2,128)(2,1)S(1)}, u32[]{:S(2)}) copy-start(bf16[4,64,2,256]{3,2,1,0:T(2,128)(2,1)S(1)} %reshape.3327) | copy-start | bytes 786436
  12.0 2.4 copy-start.12
  14.4 18.0 %copy-start.53 = (s32[128,2]{0,1:T(2,128)S(1)}, s32[128,2]{0,1:T(2,128)}, u32[]{:S(2)}) copy-start(s32[128,2]{0,1:T(2,128)} %param.27) | copy-start | bytes 3076
  31.5 1.3 copy-start.2
  31.5 2.5 copy-start.16
  39.2 63.3 %all-to-all-start = ((bf16[64,5,2048]{2,1,0:T(8,128)(2,1)}), bf16[64,5,2048]{2,1,0:T(8,128)(2,1)S(1)}, u32[]{:S(2)}, u32[]{:S(2)}) async-start(bf16[64,5,2048]{2,1,0:T(8,128)(2,1)} %broadcast_select_fusion.3), calls=%async_computation | async-start | bytes 4194304 | tf_op jit(solution)/shard_map/all_to_all | solution.py:250
  51.3 86.2 %all-gather.12.cloned.1.call-start = ((), (), s32[]{:S(2)}) async-start(), calls=%async_computation.4 | async-start | bytes 2662400 | tf_op jit(solution)/shard_map/all_gather | solution.py:59
  52.2 1.3 copy-start.40
  52.2 50.9 %copy-start.31 = (f32[2]{0:T(128)}, f32[2]{0:T(128)S(1)}, u32[]{:S(2)}) copy-start(f32[2]{0:T(128)S(1)} %get-tuple-element.244) | copy-start | bytes 28
  52.2 3.8 %copy-start.35 = (f32[2]{0:T(128)}, f32[2]{0:T(128)S(1)}, u32[]{:S(2)}) copy-start(f32[2]{0:T(128)S(1)} %get-tuple-element.324) | copy-start | bytes 28
  52.2 3.8 %copy-start.37 = (f32[2]{0:T(128)}, f32[2]{0:T(128)S(1)}, u32[]{:S(2)}) copy-start(f32[2]{0:T(128)S(1)} %get-tuple-element.325) | copy-start | bytes 28
  52.2 50.8 %copy-start.33 = (f32[2]{0:T(128)}, f32[2]{0:T(128)S(1)}, u32[]{:S(2)}) copy-start(f32[2]{0:T(128)S(1)} %get-tuple-element.299) | copy-start | bytes 28
  55.9 217.1 %all-gather.14.cloned.1.call-start = ((), (), s32[]{:S(2)}) async-start(), calls=%async_computation.5 | async-start | bytes 4792320 | tf_op jit(solution)/shard_map/all_gather | solution.py:59
  103.1 30.3 %collective-permute-start = (bf16[320,2048]{1,0:T(8,128)(2,1)S(1)}, bf16[320,2048]{1,0:T(8,128)(2,1)S(1)}, u32[]{:S(2)}, u32[]{:S(2)}) collective-permute-start(bf16[320,2048]{1,0:T(8,128)(2,1)S(1)} %all_to_all.18), channel_id=1, source_target_pairs={{0,1},{1,2},{2,3},{3,0},{4,5},{5,6},{6,7},{7,4},{8,9},{9,10},{10,1... | collective-permute-start | bytes 3932168 | tf_op jit(solution)/shard_map/ppermute | solution.py:30
  104.7 30.1 %collective-permute-start.1 = (bf16[320,2048]{1,0:T(8,128)(2,1)S(1)}, bf16[320,2048]{1,0:T(8,128)(2,1)}, u32[]{:S(2)}, u32[]{:S(2)}) collective-permute-start(bf16[320,2048]{1,0:T(8,128)(2,1)S(1)} %all_to_all.18), channel_id=1, source_target_pairs={{0,3},{1,0},{2,1},{3,2},{4,7},{5,4},{6,5},{7,6},{8,11},{9,8},{10,9... | collective-permute-start | bytes 3932168 | tf_op jit(solution)/shard_map/ppermute | solution.py:35
  133.4 29.5 %collective-permute-start.2 = (bf16[320,2048]{1,0:T(8,128)(2,1)S(1)}, bf16[320,2048]{1,0:T(8,128)(2,1)}, u32[]{:S(2)}, u32[]{:S(2)}) collective-permute-start(bf16[320,2048]{1,0:T(8,128)(2,1)S(1)} %collective-permute-done), channel_id=1, source_target_pairs={{0,1},{1,2},{2,3},{3,0},{4,5},{5,6},{6,7},{7,4},{8,9},{9,10},{10,1... | collective-permute-start | bytes 3932168 | tf_op jit(solution)/shard_map/ppermute | solution.py:30
  138.3 1.5 copy-start.42
  138.3 1.5 copy-start.45
  138.3 1.6 copy-start.47
  138.3 1.6 copy-start.49
  138.4 4.5 %copy-start.23 = (f32[2]{0:T(128)}, f32[2]{0:T(128)S(1)}, u32[]{:S(2)}) copy-start(f32[2]{0:T(128)S(1)} %get-tuple-element.239) | copy-start | bytes 28
  138.9 4.0 %copy-start.25 = (f32[2]{0:T(128)}, f32[2]{0:T(128)S(1)}, u32[]{:S(2)}) copy-start(f32[2]{0:T(128)S(1)} %get-tuple-element.289) | copy-start | bytes 28
  138.9 4.0 %copy-start.27 = (f32[2]{0:T(128)}, f32[2]{0:T(128)S(1)}, u32[]{:S(2)}) copy-start(f32[2]{0:T(128)S(1)} %get-tuple-element.290) | copy-start | bytes 28
  138.9 4.0 %copy-start.29 = (f32[2]{0:T(128)}, f32[2]{0:T(128)S(1)}, u32[]{:S(2)}) copy-start(f32[2]{0:T(128)S(1)} %get-tuple-element.291) | copy-start | bytes 28
  139.0 3.9 %copy-start.17 = (f32[2]{0:T(128)}, f32[2]{0:T(128)S(1)}, u32[]{:S(2)}) copy-start(f32[2]{0:T(128)S(1)} %get-tuple-element.296) | copy-start | bytes 28
  139.0 3.9 %copy-start.19 = (f32[2]{0:T(128)}, f32[2]{0:T(128)S(1)}, u32[]{:S(2)}) copy-start(f32[2]{0:T(128)S(1)} %get-tuple-element.297) | copy-start | bytes 28
  139.0 3.9 %copy-start.21 = (f32[2]{0:T(128)}, f32[2]{0:T(128)S(1)}, u32[]{:S(2)}) copy-start(f32[2]{0:T(128)S(1)} %get-tuple-element.298) | copy-start | bytes 28
  193.0 5.4 %copy-start.14 = (bf16[256,512]{1,0:T(8,128)(2,1)S(1)}, bf16[256,512]{1,0:T(8,128)(2,1)}, u32[]{:S(2)}) copy-start(bf16[256,512]{1,0:T(8,128)(2,1)} %param.17) | copy-start | bytes 786436
  193.0 8.2 %copy-start.1 = (f32[2,516,256]{2,1,0:T(8,128)S(1)}, f32[2,516,256]{2,1,0:T(8,128)}, u32[]{:S(2)}) copy-start(f32[2,516,256]{2,1,0:T(8,128)} %all-gather.10.cloned.1.call-done) | copy-start | bytes 3170308
  193.0 62.3 %all-to-all-start.1 = ((bf16[4,320,2048]{2,1,0:T(8,128)(2,1)}), bf16[4,320,2048]{2,1,0:T(8,128)(2,1)}, u32[]{:S(2)}, u32[]{:S(2)}) async-start(bf16[4,320,2048]{2,1,0:T(8,128)(2,1)} %bitcast.531), calls=%async_computation.1 | async-start | bytes 10485760 | tf_op jit(solution)/shard_map/all_to_all | solution.py:90
  198.2 4.1 %copy-start = (f32[4,516,256]{2,1,0:T(8,128)S(1)}, f32[4,516,256]{2,1,0:T(8,128)}, u32[]{:S(2)}) copy-start(f32[4,516,256]{2,1,0:T(8,128)} %all-gather.12.cloned.1.call-done) | copy-start | bytes 6340612
  260.6 13.5 %copy-start.39 = (f32[4,2]{1,0:T(4,128)S(1)}, f32[4,2]{1,0:T(4,128)}, u32[]{:S(2)}) copy-start(f32[4,2]{1,0:T(4,128)} %get-tuple-element.81) | copy-start | bytes 100
  260.6 13.5 %copy-start.55 = (f32[4,2]{1,0:T(4,128)S(1)}, f32[4,2]{1,0:T(4,128)}, u32[]{:S(2)}) copy-start(f32[4,2]{1,0:T(4,128)} %get-tuple-element.76) | copy-start | bytes 100
  260.6 13.7 %copy-start.41 = (f32[2]{0:T(128)S(1)}, f32[2]{0:T(128)}, u32[]{:S(2)}) copy-start(f32[2]{0:T(128)} %copy-done.40) | copy-start | bytes 28
  260.6 13.7 %copy-start.43 = (f32[2]{0:T(128)S(1)}, f32[2]{0:T(128)}, u32[]{:S(2)}) copy-start(f32[2]{0:T(128)} %copy-done.42) | copy-start | bytes 28
  260.6 13.7 %copy-start.46 = (f32[2]{0:T(128)S(1)}, f32[2]{0:T(128)}, u32[]{:S(2)}) copy-start(f32[2]{0:T(128)} %copy-done.45) | copy-start | bytes 28
  260.6 13.7 %copy-start.48 = (f32[2]{0:T(128)S(1)}, f32[2]{0:T(128)}, u32[]{:S(2)}) copy-start(f32[2]{0:T(128)} %copy-done.47) | copy-start | bytes 28
  260.7 13.7 %copy-start.50 = (f32[2]{0:T(128)S(1)}, f32[2]{0:T(128)}, u32[]{:S(2)}) copy-start(f32[2]{0:T(128)} %copy-done.49) | copy-start | bytes 28
  260.7 13.7 %copy-start.52 = (f32[2]{0:T(128)S(1)}, f32[2]{0:T(128)}, u32[]{:S(2)}) copy-start(f32[2]{0:T(128)} %copy-done.51) | copy-start | bytes 28
  260.7 13.7 %copy-start.56 = (f32[2]{0:T(128)S(1)}, f32[2]{0:T(128)}, u32[]{:S(2)}) copy-start(f32[2]{0:T(128)} %get-tuple-element.292) | copy-start | bytes 28
  260.7 13.7 %copy-start.57 = (f32[2]{0:T(128)S(1)}, f32[2]{0:T(128)}, u32[]{:S(2)}) copy-start(f32[2]{0:T(128)} %get-tuple-element.293) | copy-start | bytes 28
  260.7 13.8 %copy-start.18 = (f32[2]{0:T(128)S(1)}, f32[2]{0:T(128)}, u32[]{:S(2)}) copy-start(f32[2]{0:T(128)} %copy-done.17) | copy-start | bytes 28
  260.7 13.8 %copy-start.20 = (f32[2]{0:T(128)S(1)}, f32[2]{0:T(128)}, u32[]{:S(2)}) copy-start(f32[2]{0:T(128)} %copy-done.19) | copy-start | bytes 28
  260.7 13.8 %copy-start.22 = (f32[2]{0:T(128)S(1)}, f32[2]{0:T(128)}, u32[]{:S(2)}) copy-start(f32[2]{0:T(128)} %copy-done.21) | copy-start | bytes 28
  260.7 13.8 %copy-start.24 = (f32[2]{0:T(128)S(1)}, f32[2]{0:T(128)}, u32[]{:S(2)}) copy-start(f32[2]{0:T(128)} %copy-done.23) | copy-start | bytes 28
  260.7 13.8 %copy-start.26 = (f32[2]{0:T(128)S(1)}, f32[2]{0:T(128)}, u32[]{:S(2)}) copy-start(f32[2]{0:T(128)} %copy-done.25) | copy-start | bytes 28
  260.7 13.8 %copy-start.28 = (f32[2]{0:T(128)S(1)}, f32[2]{0:T(128)}, u32[]{:S(2)}) copy-start(f32[2]{0:T(128)} %copy-done.27) | copy-start | bytes 28
  260.8 13.8 %copy-start.30 = (f32[2]{0:T(128)S(1)}, f32[2]{0:T(128)}, u32[]{:S(2)}) copy-start(f32[2]{0:T(128)} %copy-done.29) | copy-start | bytes 28
  260.8 13.8 %copy-start.32 = (f32[2]{0:T(128)S(1)}, f32[2]{0:T(128)}, u32[]{:S(2)}) copy-start(f32[2]{0:T(128)} %copy-done.31) | copy-start | bytes 28
  260.8 13.8 %copy-start.34 = (f32[2]{0:T(128)S(1)}, f32[2]{0:T(128)}, u32[]{:S(2)}) copy-start(f32[2]{0:T(128)} %copy-done.33) | copy-start | bytes 28
  260.8 13.8 %copy-start.36 = (f32[2]{0:T(128)S(1)}, f32[2]{0:T(128)}, u32[]{:S(2)}) copy-start(f32[2]{0:T(128)} %copy-done.35) | copy-start | bytes 28
  260.8 13.8 %copy-start.38 = (f32[2]{0:T(128)S(1)}, f32[2]{0:T(128)}, u32[]{:S(2)}) copy-start(f32[2]{0:T(128)} %copy-done.37) | copy-start | bytes 28
  260.8 14.8 %copy-start.44 = (f32[4,2,256]{2,1,0:T(2,128)S(1)}, f32[4,2,256]{2,1,0:T(2,128)}, u32[]{:S(2)}) copy-start(f32[4,2,256]{2,1,0:T(2,128)} %get-tuple-element.83) | copy-start | bytes 24580
  260.8 63.5 %all-to-all-start.2 = ((bf16[64,5,2048]{2,1,0:T(8,128)(2,1)}), bf16[64,5,2048]{2,1,0:T(8,128)(2,1)S(1)}, u32[]{:S(2)}, u32[]{:S(2)}) async-start(bf16[64,5,2048]{2,1,0:T(8,128)(2,1)} %all_to_all.20), calls=%async_computation.2 | async-start | bytes 4194304 | tf_op jit(solution)/shard_map/all_to_all | solution.py:260
  278.5 2.8 copy-start.3
  278.5 2.8 copy-start.4
  278.5 2.8 copy-start.6
  278.5 2.8 copy-start.7
  278.5 2.9 copy-start.8
  278.5 3.1 copy-start.9
  281.6 1.6 copy-start.5
  281.6 1.6 copy-start.13
  283.0 1.6 copy-start.11
  (3 other events, 2.4 us)
Sparse Core Ops, SparseCore 0:
  32.5 17.2 all-gather.9
  56.1 46.2 all-gather.11
  143.0 53.0 all-gather.13
